TPU v7x, 32 devices: a whole 2x2x4 slice. The times are simulated.
32 devices in a mesh: sp: 8 (over z, x), tp: 4 (over y, core).
Axes of the slice: x: 2, y: 2, z: 4, core: 2. Of those that a mesh axis runs over, the one named last changes fastest.
Arguments:
- hidden_in: bfloat16 [2048, 2048], P('sp'), may hold values from -6 to 6
- cotangent: bfloat16 [2048, 2048], P('sp'), may hold values from -6 to 6
- routes: int32 [2048, 2], P('sp'), may hold values from 0 to 7, all different within a row; in each aligned block of 256 rows (0 to 255, 256 to 511, ...) at most 96 rows name the same one
- routing_weights: float32 [2048, 2], P('sp'), may hold values from 0.1 to 1
- w_gate: bfloat16 [8, 2048, 1024], P('sp', None, 'tp'), may hold values from -0.125 to 0.125
- w_up: bfloat16 [8, 2048, 1024], P('sp', None, 'tp'), may hold values from -0.125 to 0.125
- w_down: bfloat16 [8, 1024, 2048], P('sp', 'tp'), may hold values from -0.1875 to 0.1875
- b_gate: bfloat16 [2048, 1024], P('sp', 'tp'), may hold values from -6 to 6
- c_gate: bfloat16 [2048, 1024], P('sp', 'tp'), may hold values from -6 to 6
- x_in: bfloat16 [2048, 1024], P('sp', 'tp'), may hold values from -6 to 6
- taps: bfloat16 [3, 1024], P(None, 'tp'), may hold values from -3 to 3
- w_out: bfloat16 [2048, 1024], P(None, 'tp'), may hold values from -0.1875 to 0.1875
Outputs:
- grad_gate: bfloat16 [8, 2048, 1024], P('sp', None, 'tp')
- grad_up: bfloat16 [8, 2048, 1024], P('sp', None, 'tp')
- grad_down: bfloat16 [8, 1024, 2048], P('sp', 'tp')
- out_proj_grad: float32 [2048, 1024], P('sp', 'tp')
- residual_grad: bfloat16 [2048, 2048], P('sp', 'tp')
- grad_b: bfloat16 [2048, 1024], P('sp', 'tp')
- grad_c: bfloat16 [2048, 1024], P('sp', 'tp')
- grad_x: bfloat16 [2048, 1024], P('sp', 'tp')
Inputs may be any that keep to these rules, and one draw needn't show every extreme that they name: `routes`: each row names 2 different experts. Among the rows of one index of sp no expert is named more than 96 times, a bound that some block reaches in some of them.
All inputs are finite; a program needn't handle non-finite values.
Results may differ from a plain program's by a relative error of at most 0.01.
Values may be sent and summed in bfloat16 or wider, within the bound.
A program may use at most 64 MiB of HBM per device.

v0:
```python
import jax
import jax.numpy as jnp
from jax import lax
from jax.sharding import PartitionSpec as P


def from_behind(x, axis, by):
    devices = lax.axis_size(axis)
    pairs = [(i, i + by) for i in range(devices) if 0 <= i + by < devices]
    return lax.ppermute(x, axis, pairs)


def per_device(
    hidden_in,
    cotangent,
    routes,
    routing_weights,
    w_gate,
    w_up,
    w_down,
    b_gate,
    c_gate,
    x_in,
    taps,
    w_out,
):
    tok_rows, model_width = hidden_in.shape
    top_k = routes.shape[1]
    local_experts = w_gate.shape[0]
    sp_size = lax.axis_size("sp")
    tp_size = lax.axis_size("tp")
    experts = local_experts * sp_size
    capacity = 3 * tok_rows * top_k // (2 * experts)
    slot_count = tok_rows * top_k
    feature_share = model_width // tp_size
    share_offset = lax.axis_index("tp") * feature_share
    flat_ids = routes.reshape(-1)
    onehot = (flat_ids[:, None] == jnp.arange(experts, dtype=jnp.int32)[None, :]).astype(jnp.int32)
    before = jnp.cumsum(onehot, axis=0) - onehot
    position = jnp.sum(before * onehot, axis=1)
    target = flat_ids * capacity + position
    source = (
        jnp.full((experts * capacity,), slot_count, jnp.int32)
        .at[target]
        .set(jnp.arange(slot_count, dtype=jnp.int32))
    )
    filled = source < slot_count
    clipped = jnp.minimum(source, slot_count - 1)
    token_of = clipped // top_k
    weight_of = jnp.where(filled, routing_weights.reshape(-1)[clipped], 0.0)
    rows_src = lax.dynamic_slice_in_dim(hidden_in, share_offset, feature_share, 1)
    cot_src = lax.dynamic_slice_in_dim(cotangent, share_offset, feature_share, 1)
    send_rows = jnp.where(filled[:, None], rows_src[token_of], jnp.zeros((), jnp.bfloat16))
    send_rows = send_rows.reshape(experts, capacity, -1)
    send_cot = (weight_of[:, None] * cot_src[token_of].astype(jnp.float32)).astype(jnp.bfloat16)
    send_cot = send_cot.reshape(experts, capacity, -1)
    part_rows, part_cot = (
        lax.all_to_all(send_rows, "sp", split_axis=0, concat_axis=1, tiled=True),
        lax.all_to_all(send_cot, "sp", split_axis=0, concat_axis=1, tiled=True),
    )
    rows_h, rows_s = (
        lax.all_gather(part_rows, "tp", axis=2, tiled=True),
        lax.all_gather(part_cot, "tp", axis=2, tiled=True),
    )
    pre_gate = jnp.einsum("erd,edf->erf", rows_h, w_gate, preferred_element_type=jnp.float32)
    pre_up = jnp.einsum("erd,edf->erf", rows_h, w_up, preferred_element_type=jnp.float32)
    sigma = jax.nn.sigmoid(pre_gate)
    silu_gate = pre_gate * sigma
    hid = (silu_gate * pre_up).astype(jnp.bfloat16)
    d_hid = jnp.einsum("erd,efd->erf", rows_s, w_down, preferred_element_type=jnp.float32)
    d_up = (d_hid * silu_gate).astype(jnp.bfloat16)
    d_pre = (d_hid * pre_up * sigma * (1.0 + pre_gate * (1.0 - sigma))).astype(jnp.bfloat16)
    grad_down = jnp.einsum("erf,erd->efd", hid, rows_s, preferred_element_type=jnp.float32).astype(
        jnp.bfloat16
    )
    grad_gate = jnp.einsum(
        "erd,erf->edf", rows_h, d_pre, preferred_element_type=jnp.float32
    ).astype(jnp.bfloat16)
    grad_up = jnp.einsum("erd,erf->edf", rows_h, d_up, preferred_element_type=jnp.float32).astype(
        jnp.bfloat16
    )
    partial_grad = jnp.einsum("erf,edf->erd", d_pre, w_gate, preferred_element_type=jnp.float32)
    partial_grad = partial_grad + jnp.einsum(
        "erf,edf->erd", d_up, w_up, preferred_element_type=jnp.float32
    )
    partial_low = partial_grad.astype(jnp.bfloat16)
    shared_rows = (
        lax.psum_scatter(partial_low, "tp", scatter_dimension=2, tiled=True)
        .astype(jnp.float32)
        .astype(jnp.bfloat16)
    )
    back = lax.all_to_all(shared_rows, "sp", split_axis=1, concat_axis=0, tiled=True)
    back_flat = back.reshape(experts * capacity, feature_share)
    per_token = back_flat[target].astype(jnp.float32).reshape(tok_rows, top_k, feature_share)
    own_cot = lax.dynamic_slice_in_dim(cotangent, share_offset, feature_share, 1).astype(
        jnp.float32
    )
    residual_grad = (own_cot + jnp.sum(per_token, axis=1)).astype(jnp.bfloat16)
    full_grad = lax.all_gather(residual_grad, "tp", axis=1, tiled=True)
    taps_f = taps.astype(jnp.float32)
    gated = c_gate.astype(jnp.float32) * x_in.astype(jnp.float32)
    earlier = from_behind(gated[tok_rows - 2 :], "sp", 1)
    padded = jnp.concatenate([earlier, gated], axis=0)
    conv = (
        taps_f[0] * padded[0:tok_rows]
        + taps_f[1] * padded[1 : tok_rows + 1]
        + taps_f[2] * padded[2 : tok_rows + 2]
    )
    b_f = b_gate.astype(jnp.float32)
    y_short = (b_f * conv).astype(jnp.bfloat16)
    d_y = jnp.dot(full_grad, w_out, preferred_element_type=jnp.float32)
    grad_b = (d_y * conv).astype(jnp.bfloat16)
    d_conv = b_f * d_y
    following = from_behind(d_conv[0:2], "sp", -1)
    later = jnp.concatenate([d_conv, following], axis=0)
    d_v = (
        taps_f[2] * later[0:tok_rows]
        + taps_f[1] * later[1 : tok_rows + 1]
        + taps_f[0] * later[2 : tok_rows + 2]
    )
    grad_c = (d_v * x_in.astype(jnp.float32)).astype(jnp.bfloat16)
    grad_x = (d_v * c_gate.astype(jnp.float32)).astype(jnp.bfloat16)
    out_proj_grad = lax.psum_scatter(
        jnp.einsum("td,tc->dc", full_grad, y_short, preferred_element_type=jnp.float32),
        "sp",
        scatter_dimension=0,
        tiled=True,
    )
    return (grad_gate, grad_up, grad_down, out_proj_grad, residual_grad, grad_b, grad_c, grad_x)


def solution(mesh):
    return jax.shard_map(
        per_device,
        mesh=mesh,
        in_specs=(
            P("sp", None),
            P("sp", None),
            P("sp", None),
            P("sp", None),
            P("sp", None, "tp"),
            P("sp", None, "tp"),
            P("sp", "tp", None),
            P("sp", "tp"),
            P("sp", "tp"),
            P("sp", "tp"),
            P(None, "tp"),
            P(None, "tp"),
        ),
        out_specs=(
            P("sp", None, "tp"),
            P("sp", None, "tp"),
            P("sp", "tp", None),
            P("sp", "tp"),
            P("sp", "tp"),
            P("sp", "tp"),
            P("sp", "tp"),
            P("sp", "tp"),
        ),
        check_vma=False,
    )
```

profile of v0, /device:TPU:0, one launch (start us, length us, event | category | flops | bytes accessed | tf_op | source)
XLA Modules:
  0.0 290.6 jit_solution(8759638803570472328)
XLA Ops:
  7.2 0.8 broadcast_multiply_fusion
  8.0 0.8 copy.30
  9.4 1.1 reduce-window.6
  10.6 0.2 slice_reduce_fusion
  10.9 2.4 scatter_custom_fusion
  13.4 0.8 copy.32
  14.4 5.0 %gather_fusion.1 = f32[768]{0:T(1024)S(1)} fusion(f32[512]{0:T(512)S(1)} %reshape.162, s32[1024]{0:T(1024)S(1)} %get-tuple-element.22), kind=kCustom, calls=%fused_computation.1 | custom fusion | bytes 9216 | tf_op jit(solution)/shard_map/gather | solution.py:50
  19.5 1.0 constant_dynamic-slice_fusion.1
  20.5 2.7 gather_fusion
  23.3 27.3 %all_to_all.33 = bf16[8,96,512]{2,1,0:T(8,128)(2,1)} all-to-all(bf16[8,96,512]{2,1,0:T(8,128)(2,1)S(1)} %broadcast_select_fusion), channel_id=1, replica_groups=mesh['sp'=8,'tp'=4] {'sp'}, dimensions={0} | all-to-all | bytes 1572864 | tf_op jit(solution)/shard_map/all_to_all | solution.py:58
  50.7 1.0 constant_dynamic-slice_fusion
  51.7 2.7 gather_fusion.2
  54.5 0.2 fusion.31
  54.7 23.3 %all_to_all.34 = bf16[8,96,512]{2,1,0:T(8,128)(2,1)} all-to-all(bf16[8,96,512]{2,1,0:T(8,128)(2,1)S(1)} %fusion.31), channel_id=1, replica_groups=mesh['sp'=8,'tp'=4] {'sp'}, dimensions={0} | all-to-all | bytes 1572864 | tf_op jit(solution)/shard_map/all_to_all | solution.py:59
  78.0 0.2 reduce-scatter.3.cloned.1.call-start
  78.4 3.9 %fusion.8 = f32[768,256]{1,0:T(8,128)} fusion(bf16[1,768,2048]{2,1,0:T(8,128)(2,1)} %all-gather.4.cloned.1.call-done, bf16[1,2048,256]{2,1,0:T(8,128)(2,1)S(1)} %copy-done), kind=kOutput, calls=%fused_computation.14 | convolution fusion | flops 805306368 | bytes 4980736 | tf_op jit(solution)/shard_map/erd,edf->erf/dot_general | solution.py:65
  82.3 1.9 fusion.10
  84.2 24.3 %all-gather.6.cloned.1.call-done = bf16[1,768,2048]{2,1,0:T(8,128)(2,1)} async-done(((bf16[1,768,512]{2,1,0:T(8,128)(2,1)}), bf16[1,768,2048]{2,1,0:T(8,128)(2,1)}) %all-gather.6.cloned.1.call-update) | async-done | bytes 3145744 | tf_op jit(solution)/shard_map/all_gather | solution.py:63
  108.5 3.5 %multiply_convert_fusion.1 = (bf16[768,256]{1,0:T(8,128)(2,1)S(1)}, bf16[768,256]{1,0:T(8,128)(2,1)S(1)}) fusion(f32[768,256]{1,0:T(8,128)} %fusion.8, f32[768,256]{1,0:T(8,128)} %fusion.10, bf16[1,256,2048]{2,1,0:T(8,128)(2,1)S(1)} %copy-done.14, bf16[1,768,2048]{2,1,0:T(8,128)(2,1)} %all-gather.6.cloned.1.call-done), kind=kOutput, calls=%fused_computation.35 | convolution fusion | flops 807862272 | bytes 6553600 | tf_op jit(solution)/shard_map/erd,efd->erf/dot_general | solution.py:70
  112.0 1.0 fusion.32
  113.0 2.7 fusion.12
  115.8 37.9 %reduce-scatter.3.cloned.1.call-done = bf16[1,768,512]{2,1,0:T(8,128)(2,1)} async-done(((bf16[1,768,2048]{2,1,0:T(8,128)(2,1)}), bf16[1,768,512]{2,1,0:T(8,128)(2,1)}) %reduce-scatter.3.cloned.1.call-update) | async-done | bytes 786448 | tf_op jit(solution)/shard_map/reduce_scatter | solution.py:88
  153.7 2.3 copy.38
  156.0 0.5 broadcast.111
  156.5 5.6 %reduce.2 = bf16[768,512]{1,0:T(8,128)(2,1)S(1)} reduce(bf16[768,1,512]{2,1,0:T(2,128)(2,1)S(1)} %bitcast.84, bf16[]{:T(256)} %broadcast.111), dimensions={1}, to_apply=%bitcast.82.reduce_sub_computation | reduce | bytes 1572866
  162.2 1.5 reshape.216
  163.6 5.5 %all-to-all-start.2 = ((bf16[8,2,24576]{2,1,0:T(2,128)(2,1)}), bf16[8,2,24576]{2,1,0:T(2,128)(2,1)S(1)}, u32[]{:S(2)}, u32[]{:S(2)}) async-start(bf16[8,2,24576]{2,1,0:T(2,128)(2,1)} %reshape.216), calls=%async_computation.3 | async-start | bytes 1572864 | tf_op jit(solution)/shard_map/all_to_all | solution.py:92
  169.1 0.3 all-gather.8.cloned.1.call-start
  169.4 19.8 %all-to-all-done.2 = bf16[8,2,24576]{2,1,0:T(2,128)(2,1)S(1)} async-done(((bf16[8,2,24576]{2,1,0:T(2,128)(2,1)}), bf16[8,2,24576]{2,1,0:T(2,128)(2,1)S(1)}, u32[]{:S(2)}, u32[]{:S(2)}) %all-to-all-start.2) | async-done | bytes 786464 | tf_op jit(solution)/shard_map/all_to_all | solution.py:92
  189.2 0.8 reshape.217
  190.0 0.2 copy.37
  190.2 2.0 gather_fusion.3
  192.3 0.7 reshape.169
  192.9 1.2 reduce_sum.22
  194.2 1.7 add_convert_fusion.1
  196.0 3.2 %collective-permute-start = (f32[2,256]{1,0:T(2,128)S(1)}, f32[2,256]{1,0:T(2,128)S(1)}, u32[]{:S(2)}, u32[]{:S(2)}) collective-permute-start(f32[2,256]{1,0:T(2,128)S(1)} %slice.57), channel_id=1, source_target_pairs={{0,4},{4,8},{8,12},{12,16},{16,20},{20,24},{24,28},{1,5},{5,9},{9,... | collective-permute-start | bytes 6152 | tf_op jit(solution)/shard_map/ppermute | solution.py:10
  199.3 1.3 collective-permute-done
  200.6 10.2 %all-gather.8.cloned.1.call-done = bf16[256,2048]{1,0:T(8,128)(2,1)} async-done(((bf16[256,512]{1,0:T(8,128)(2,1)}), bf16[256,2048]{1,0:T(8,128)(2,1)}) %all-gather.8.cloned.1.call-update) | async-done | bytes 1048592 | tf_op jit(solution)/shard_map/all_gather | solution.py:99
  210.8 2.7 multiply_convert_fusion.4
  213.5 1.8 fusion.53
  215.4 4.1 %fusion.28 = bf16[1,2048,256]{2,1,0:T(8,128)(2,1)} fusion(bf16[768,256]{1,0:T(8,128)(2,1)S(1)} %copy-done.2, bf16[1,768,2048]{2,1,0:T(8,128)(2,1)} %all-gather.4.cloned.1.call-done), kind=kOutput, calls=%fused_computation.24 | convolution fusion | flops 805830656 | bytes 4587520 | tf_op jit(solution)/shard_map/erd,erf->edf/dot_general | solution.py:76
  219.5 2.0 fusion.22
  221.5 1.3 collective-permute-start.1
  222.9 2.0 fusion.25
  224.9 2.3 collective-permute-done.1
  227.2 0.8 fusion.48
  227.9 0.7 fusion.49
  228.6 55.5 %reduce-scatter.5.cloned.1.call-done = f32[256,256]{1,0:T(8,128)} async-done(((f32[2048,256]{1,0:T(8,128)}), f32[256,256]{1,0:T(8,128)}) %reduce-scatter.5.cloned.1.call-update) | async-done | bytes 262160 | tf_op jit(solution)/shard_map/reduce_scatter | solution.py:123
  (65 shorter events, 1.7 us)
Async XLA Ops:
  7.2 71.2 %copy-start = (bf16[1,2048,256]{2,1,0:T(8,128)(2,1)S(1)}, bf16[1,2048,256]{2,1,0:T(8,128)(2,1)}, u32[]{:S(2)}) copy-start(bf16[1,2048,256]{2,1,0:T(8,128)(2,1)} %param.16) | copy-start | bytes 3145732
  7.2 71.2 %all-gather.4.cloned.1.call-start = ((), (), s32[]{:S(2)}) async-start(), calls=%async_computation.5 | async-start | bytes 3932160 | tf_op jit(solution)/shard_map/all_gather | solution.py:62
  50.7 57.8 %all-gather.6.cloned.1.call-start = ((), (), s32[]{:S(2)}) async-start(), calls=%async_computation.6 | async-start | bytes 3932160 | tf_op jit(solution)/shard_map/all_gather | solution.py:63
  78.0 4.3 %copy-start.4 = (bf16[1,2048,256]{2,1,0:T(8,128)(2,1)S(1)}, bf16[1,2048,256]{2,1,0:T(8,128)(2,1)}, u32[]{:S(2)}) copy-start(bf16[1,2048,256]{2,1,0:T(8,128)(2,1)} %param.17) | copy-start | bytes 3145732
  78.0 75.6 %reduce-scatter.3.cloned.1.call-start = ((), (), s32[]{:S(2)}) async-start(), calls=%async_computation.7 | async-start | bytes 3932160 | tf_op jit(solution)/shard_map/reduce_scatter | solution.py:88
  78.4 3.9 %copy-start.11 = (bf16[1,768,2048]{2,1,0:T(8,128)(2,1)S(1)}, bf16[1,768,2048]{2,1,0:T(8,128)(2,1)}, u32[]{:S(2)}) copy-start(bf16[1,768,2048]{2,1,0:T(8,128)(2,1)} %all-gather.4.cloned.1.call-done) | copy-start | bytes 9437188
  82.3 26.2 %copy-start.14 = (bf16[1,256,2048]{2,1,0:T(8,128)(2,1)S(1)}, bf16[1,256,2048]{2,1,0:T(8,128)(2,1)}, u32[]{:S(2)}) copy-start(bf16[1,256,2048]{2,1,0:T(8,128)(2,1)} %param.18) | copy-start | bytes 3145732
  112.0 1.0 copy-start.1
  112.0 1.0 copy-start.7
  163.6 25.6 %all-to-all-start.2 = ((bf16[8,2,24576]{2,1,0:T(2,128)(2,1)}), bf16[8,2,24576]{2,1,0:T(2,128)(2,1)S(1)}, u32[]{:S(2)}, u32[]{:S(2)}) async-start(bf16[8,2,24576]{2,1,0:T(2,128)(2,1)} %reshape.216), calls=%async_computation.3 | async-start | bytes 1572864 | tf_op jit(solution)/shard_map/all_to_all | solution.py:92
  169.1 41.6 %all-gather.8.cloned.1.call-start = ((), (), s32[]{:S(2)}) async-start(), calls=%async_computation.8 | async-start | bytes 1310720 | tf_op jit(solution)/shard_map/all_gather | solution.py:99
  192.2 3.8 %copy-start.5 = (bf16[256,256]{1,0:T(8,128)(2,1)S(1)}, bf16[256,256]{1,0:T(8,128)(2,1)}, u32[]{:S(2)}) copy-start(bf16[256,256]{1,0:T(8,128)(2,1)} %param.20) | copy-start | bytes 393220
  192.2 3.8 %copy-start.6 = (bf16[256,256]{1,0:T(8,128)(2,1)S(1)}, bf16[256,256]{1,0:T(8,128)(2,1)}, u32[]{:S(2)}) copy-start(bf16[256,256]{1,0:T(8,128)(2,1)} %param.21) | copy-start | bytes 393220
  192.2 7.0 %copy-start.10 = (bf16[3,256]{1,0:T(4,128)(2,1)S(1)}, bf16[3,256]{1,0:T(4,128)(2,1)}, u32[]{:S(2)}) copy-start(bf16[3,256]{1,0:T(4,128)(2,1)} %param.22) | copy-start | bytes 4612
  192.3 18.5 %copy-start.9 = (bf16[256,256]{1,0:T(8,128)(2,1)S(1)}, bf16[256,256]{1,0:T(8,128)(2,1)}, u32[]{:S(2)}) copy-start(bf16[256,256]{1,0:T(8,128)(2,1)} %param.19) | copy-start | bytes 393220
  195.9 88.1 %reduce-scatter.5.cloned.1.call-start = ((), (), s32[]{:S(2)}) async-start(), calls=%async_computation.9 | async-start | bytes 2359296 | tf_op jit(solution)/shard_map/reduce_scatter | solution.py:123
  196.0 4.5 %collective-permute-start = (f32[2,256]{1,0:T(2,128)S(1)}, f32[2,256]{1,0:T(2,128)S(1)}, u32[]{:S(2)}, u32[]{:S(2)}) collective-permute-start(f32[2,256]{1,0:T(2,128)S(1)} %slice.57), channel_id=1, source_target_pairs={{0,4},{4,8},{8,12},{12,16},{16,20},{20,24},{24,28},{1,5},{5,9},{9,... | collective-permute-start | bytes 6152 | tf_op jit(solution)/shard_map/ppermute | solution.py:10
  210.8 2.7 copy-start.3
  213.5 1.9 copy-start.2
  215.4 4.1 %copy-start.13 = (bf16[1,768,2048]{2,1,0:T(8,128)(2,1)S(1)}, bf16[1,768,2048]{2,1,0:T(8,128)(2,1)}, u32[]{:S(2)}) copy-start(bf16[1,768,2048]{2,1,0:T(8,128)(2,1)} %all-gather.6.cloned.1.call-done) | copy-start | bytes 9437188
  215.4 4.1 %copy-start.15 = (f32[768,256]{1,0:T(8,128)S(1)}, f32[768,256]{1,0:T(8,128)}, u32[]{:S(2)}) copy-start(f32[768,256]{1,0:T(8,128)} %fusion.8) | copy-start | bytes 2359300
  215.4 4.1 %copy-start.16 = (f32[768,256]{1,0:T(8,128)S(1)}, f32[768,256]{1,0:T(8,128)}, u32[]{:S(2)}) copy-start(f32[768,256]{1,0:T(8,128)} %fusion.10) | copy-start | bytes 2359300
  219.5 3.3 %copy-start.8 = (bf16[768,256]{1,0:T(8,128)(2,1)S(1)}, bf16[768,256]{1,0:T(8,128)(2,1)}, u32[]{:S(2)}) copy-start(bf16[768,256]{1,0:T(8,128)(2,1)} %copy-done.7) | copy-start | bytes 1179652
  219.5 3.3 %copy-start.12 = (bf16[1,768,2048]{2,1,0:T(8,128)(2,1)S(1)}, bf16[1,768,2048]{2,1,0:T(8,128)(2,1)}, u32[]{:S(2)}) copy-start(bf16[1,768,2048]{2,1,0:T(8,128)(2,1)} %all-gather.4.cloned.1.call-done) | copy-start | bytes 9437188
  221.5 5.6 %collective-permute-start.1 = (f32[2,256]{1,0:T(2,128)S(1)}, f32[2,256]{1,0:T(2,128)S(1)}, u32[]{:S(2)}, u32[]{:S(2)}) collective-permute-start(f32[2,256]{1,0:T(2,128)S(1)} %slice.62), channel_id=1, source_target_pairs={{4,0},{8,4},{12,8},{16,12},{20,16},{24,20},{28,24},{5,1},{9,5},{13... | collective-permute-start | bytes 6152 | tf_op jit(solution)/shard_map/ppermute | solution.py:10
Sparse Core Ops, SparseCore 0:
  50.8 27.5 all-gather.3
  80.0 28.4 all-gather.5
  115.9 37.7 reduce-scatter.2
  196.1 14.6 all-gather.7
  215.5 68.5 reduce-scatter.4
where the time goes:
time: 291 us
  waiting for transfers between devices  151 us (52%)
  blocking collectives  50.6 us (17%)
  matrix products  25.7 us (9%)
  local copies, waits for them, and re-layouts  25.5 us (9%)
  between operations  14.2 us (5%)
  other arithmetic  12.6 us (4%)
  starting transfers between devices  10.6 us (4%)
    reduce_scatter x1, waiting for transfers between devices, per_device(): lax.psum_scatter(jnp.einsum('td,tc->dc', full_grad, y_short, preferred_el...  55.5 us
    reduce_scatter x1, waiting for transfers between devices, per_device(): lax.psum_scatter(partial_low, 'tp', scatter_dimension=2, tiled=True)  37.9 us
    all_to_all x1, blocking collectives, per_device(): lax.all_to_all(send_rows, 'sp', split_axis=0, concat_axis=1, tiled=True)  27.3 us
    all_gather x1, waiting for transfers between devices, per_device(): lax.all_gather(part_cot, 'tp', axis=2, tiled=True)  24.3 us
    all_to_all x1, blocking collectives, per_device(): lax.all_to_all(send_cot, 'sp', split_axis=0, concat_axis=1, tiled=True)  23.3 us
    all_to_all x1, waiting for transfers between devices, per_device(): lax.all_to_all(shared_rows, 'sp', split_axis=1, concat_axis=0, tiled=True)  19.8 us
    all_gather x1, waiting for transfers between devices, per_device(): full_grad = lax.all_gather(residual_grad, 'tp', axis=1, tiled=True)  10.2 us
  transfers between devices with their start and end apart: 8, of which 8 were waited for; matrix products, arithmetic and copies ran while one was open for 7% of the time, Pallas kernels for 0%

commit v1 on v0

--- a/solution.py
+++ b/solution.py
@@ -58,9 +58,13 @@
         lax.all_to_all(send_rows, "sp", split_axis=0, concat_axis=1, tiled=True),
         lax.all_to_all(send_cot, "sp", split_axis=0, concat_axis=1, tiled=True),
     )
+    run_things = lambda sample, device_axis: jnp.concatenate(
+        jax.lax.all_to_all(jnp.stack(jax.lax.axis_size(device_axis) * [sample]), device_axis, 0, 0),
+        axis=2,
+    )
     rows_h, rows_s = (
         lax.all_gather(part_rows, "tp", axis=2, tiled=True),
-        lax.all_gather(part_cot, "tp", axis=2, tiled=True),
+        run_things(part_cot, "tp"),
     )
     pre_gate = jnp.einsum("erd,edf->erf", rows_h, w_gate, preferred_element_type=jnp.float32)
     pre_up = jnp.einsum("erd,edf->erf", rows_h, w_up, preferred_element_type=jnp.float32)

time: 291 us -> 302 us (1.038)
  starting transfers between devices: 10.6 us -> 15.2 us
    all_to_all x0 -> x1, waiting for transfers between devices: none -> 30.9 us  [per_device(): jax.lax.all_to_all(jnp.stack(jax.lax.axis_size(device_axis) * [sample]),...]
    all_gather x1 -> x0, waiting for transfers between devices: 24.3 us -> none  [per_device(): lax.all_gather(part_cot, 'tp', axis=2, tiled=True)]
    all_to_all x0 -> x1, starting transfers between devices: none -> 4.66 us  [per_device(): jax.lax.all_to_all(jnp.stack(jax.lax.axis_size(device_axis) * [sample]),...]
  transfers between devices with their start and end apart: 8 -> 8, of which waited for: 8 -> 7; matrix products, arithmetic and copies ran while one was open for 7% -> 8% of each run, Pallas kernels for 0% -> 0%
where the time goes in v1:
time: 302 us
  waiting for transfers between devices  154 us (51%)
  blocking collectives  50.5 us (17%)
  local copies, waits for them, and re-layouts  27.7 us (9%)
  matrix products  27.7 us (9%)
  starting transfers between devices  15.2 us (5%)
  between operations  14.2 us (5%)
  other arithmetic  12.6 us (4%)
    reduce_scatter x1, waiting for transfers between devices, per_device(): lax.psum_scatter(jnp.einsum('td,tc->dc', full_grad, y_short, preferred_el...  53.4 us
    reduce_scatter x1, waiting for transfers between devices, per_device(): lax.psum_scatter(partial_low, 'tp', scatter_dimension=2, tiled=True)  35.9 us
    all_to_all x1, waiting for transfers between devices, per_device(): jax.lax.all_to_all(jnp.stack(jax.lax.axis_size(device_axis) * [sample]),...  30.9 us
    all_to_all x1, blocking collectives, per_device(): lax.all_to_all(send_rows, 'sp', split_axis=0, concat_axis=1, tiled=True)  27.3 us
    all_to_all x1, blocking collectives, per_device(): lax.all_to_all(send_cot, 'sp', split_axis=0, concat_axis=1, tiled=True)  23.2 us
    all_to_all x1, waiting for transfers between devices, per_device(): lax.all_to_all(shared_rows, 'sp', split_axis=1, concat_axis=0, tiled=True)  19.8 us
    all_gather x1, waiting for transfers between devices, per_device(): full_grad = lax.all_gather(residual_grad, 'tp', axis=1, tiled=True)  10.2 us
  transfers between devices with their start and end apart: 8, of which 7 were waited for; matrix products, arithmetic and copies ran while one was open for 8% of the time, Pallas kernels for 0%

profile of v1, /device:TPU:0, one launch (start us, length us, event | category | flops | bytes accessed | tf_op | source)
XLA Modules:
  0.0 301.7 jit_solution(3290082321231452155)
XLA Ops:
  7.2 0.8 broadcast_multiply_fusion
  8.0 0.8 copy.33
  9.4 1.1 reduce-window.6
  10.9 2.4 scatter_custom_fusion
  13.4 0.8 copy.35
  14.4 5.0 %gather_fusion.1 = f32[768]{0:T(1024)S(1)} fusion(f32[512]{0:T(512)S(1)} %reshape.173, s32[1024]{0:T(1024)S(1)} %get-tuple-element.22), kind=kCustom, calls=%fused_computation.1 | custom fusion | bytes 9216 | tf_op jit(solution)/shard_map/gather | solution.py:50
  19.5 1.0 constant_dynamic-slice_fusion.1
  20.5 2.7 gather_fusion
  23.3 27.3 %all_to_all.35 = bf16[8,96,512]{2,1,0:T(8,128)(2,1)} all-to-all(bf16[8,96,512]{2,1,0:T(8,128)(2,1)S(1)} %broadcast_select_fusion), channel_id=1, replica_groups=mesh['sp'=8,'tp'=4] {'sp'}, dimensions={0} | all-to-all | bytes 1572864 | tf_op jit(solution)/shard_map/all_to_all | solution.py:58
  50.7 1.0 constant_dynamic-slice_fusion
  51.7 2.7 gather_fusion.2
  54.4 0.2 fusion.22
  54.7 23.2 %all_to_all.36 = bf16[8,96,512]{2,1,0:T(8,128)(2,1)S(1)} all-to-all(bf16[8,96,512]{2,1,0:T(8,128)(2,1)S(1)} %fusion.22), channel_id=1, replica_groups=mesh['sp'=8,'tp'=4] {'sp'}, dimensions={0} | all-to-all | bytes 1572864 | tf_op jit(solution)/shard_map/all_to_all | solution.py:59
  77.9 0.3 copy.36
  78.1 1.9 stack.10
  80.1 4.7 %all-to-all-start.2 = ((bf16[4,1,768,512]{2,3,1,0:T(8,128)(2,1)}), bf16[4,1,768,512]{2,3,1,0:T(8,128)(2,1)}, u32[]{:S(2)}, u32[]{:S(2)}) async-start(bf16[4,1,768,512]{2,3,1,0:T(8,128)(2,1)} %stack.10), calls=%async_computation.2 | async-start | bytes 6291456 | tf_op jit(solution)/shard_map/all_to_all | solution.py:62
  85.0 3.9 %fusion.4 = f32[768,256]{1,0:T(8,128)} fusion(bf16[1,768,2048]{2,1,0:T(8,128)(2,1)} %all-gather.3.cloned.1.call-done, bf16[1,2048,256]{2,1,0:T(8,128)(2,1)S(1)} %copy-done), kind=kOutput, calls=%fused_computation.10 | convolution fusion | flops 805306368 | bytes 4980736 | tf_op jit(solution)/shard_map/erd,edf->erf/dot_general | solution.py:69
  88.9 1.9 fusion.6
  90.8 30.9 %all-to-all-done.2 = bf16[4,1,768,512]{2,3,1,0:T(8,128)(2,1)} async-done(((bf16[4,1,768,512]{2,3,1,0:T(8,128)(2,1)}), bf16[4,1,768,512]{2,3,1,0:T(8,128)(2,1)}, u32[]{:S(2)}, u32[]{:S(2)}) %all-to-all-start.2) | async-done | bytes 3145760 | tf_op jit(solution)/shard_map/all_to_all | solution.py:62
  121.7 3.5 %multiply_convert_fusion.1 = (bf16[768,256]{1,0:T(8,128)(2,1)S(1)}, bf16[768,256]{1,0:T(8,128)(2,1)S(1)}) fusion(f32[768,256]{1,0:T(8,128)} %fusion.4, f32[768,256]{1,0:T(8,128)} %fusion.6, bf16[768,2048]{0,1:T(8,128)(2,1)} %bitcast.11, bf16[1,256,2048]{2,1,0:T(8,128)(2,1)S(1)} %copy-done.13), kind=kOutput, calls=%fused_computation.32 | convolution fusion | flops 807862272 | bytes 6553600 | tf_op jit(solution)/shard_map/erd,efd->erf/dot_general | solution.py:74
  125.2 1.0 fusion.23
  126.2 2.7 fusion.8
  129.0 35.9 %reduce-scatter.3.cloned.1.call-done = bf16[1,768,512]{2,1,0:T(8,128)(2,1)} async-done(((bf16[1,768,2048]{2,1,0:T(8,128)(2,1)}), bf16[1,768,512]{2,1,0:T(8,128)(2,1)}) %reduce-scatter.3.cloned.1.call-update) | async-done | bytes 786448 | tf_op jit(solution)/shard_map/reduce_scatter | solution.py:92
  165.0 2.3 copy.43
  167.3 0.5 broadcast.113
  167.8 5.6 %reduce.2 = bf16[768,512]{1,0:T(8,128)(2,1)S(1)} reduce(bf16[768,1,512]{2,1,0:T(2,128)(2,1)S(1)} %bitcast.80, bf16[]{:T(256)} %broadcast.113), dimensions={1}, to_apply=%bitcast.78.reduce_sub_computation | reduce | bytes 1572866
  173.5 1.5 reshape.228
  174.9 5.5 %all-to-all-start.3 = ((bf16[8,2,24576]{2,1,0:T(2,128)(2,1)}), bf16[8,2,24576]{2,1,0:T(2,128)(2,1)S(1)}, u32[]{:S(2)}, u32[]{:S(2)}) async-start(bf16[8,2,24576]{2,1,0:T(2,128)(2,1)} %reshape.228), calls=%async_computation.4 | async-start | bytes 1572864 | tf_op jit(solution)/shard_map/all_to_all | solution.py:96
  180.4 0.3 all-gather.5.cloned.1.call-start
  180.7 19.8 %all-to-all-done.3 = bf16[8,2,24576]{2,1,0:T(2,128)(2,1)S(1)} async-done(((bf16[8,2,24576]{2,1,0:T(2,128)(2,1)}), bf16[8,2,24576]{2,1,0:T(2,128)(2,1)S(1)}, u32[]{:S(2)}, u32[]{:S(2)}) %all-to-all-start.3) | async-done | bytes 786464 | tf_op jit(solution)/shard_map/all_to_all | solution.py:96
  200.5 0.8 reshape.229
  201.5 2.0 gather_fusion.3
  203.6 0.7 reshape.181
  204.2 1.2 reduce_sum.22
  205.5 1.7 add_convert_fusion.1
  207.3 3.2 %collective-permute-start = (f32[2,256]{1,0:T(2,128)S(1)}, f32[2,256]{1,0:T(2,128)S(1)}, u32[]{:S(2)}, u32[]{:S(2)}) collective-permute-start(f32[2,256]{1,0:T(2,128)S(1)} %slice.57), channel_id=1, source_target_pairs={{0,4},{4,8},{8,12},{12,16},{16,20},{20,24},{24,28},{1,5},{5,9},{9,... | collective-permute-start | bytes 6152 | tf_op jit(solution)/shard_map/ppermute | solution.py:10
  210.6 1.3 collective-permute-done
  211.9 10.2 %all-gather.5.cloned.1.call-done = bf16[256,2048]{1,0:T(8,128)(2,1)} async-done(((bf16[256,512]{1,0:T(8,128)(2,1)}), bf16[256,2048]{1,0:T(8,128)(2,1)}) %all-gather.5.cloned.1.call-update) | async-done | bytes 1048592 | tf_op jit(solution)/shard_map/all_gather | solution.py:103
  222.1 2.7 multiply_convert_fusion.4
  224.8 1.8 fusion.45
  226.7 4.0 %fusion.19 = bf16[1,2048,256]{2,1,0:T(8,128)(2,1)} fusion(bf16[768,256]{1,0:T(8,128)(2,1)S(1)} %copy-done.2, bf16[1,768,2048]{2,1,0:T(8,128)(2,1)} %all-gather.3.cloned.1.call-done), kind=kOutput, calls=%fused_computation.20 | convolution fusion | flops 805830656 | bytes 4587520 | tf_op jit(solution)/shard_map/erd,erf->edf/dot_general | solution.py:80
  230.7 4.1 %fusion.15 = bf16[1,256,2048]{2,1,0:T(8,128)(2,1)} fusion(bf16[768,2048]{0,1:T(8,128)(2,1)} %bitcast.11, f32[768,256]{1,0:T(8,128)S(1)} %copy-done.15, f32[768,256]{1,0:T(8,128)S(1)} %copy-done.14), kind=kOutput, calls=%fused_computation.18 | convolution fusion | flops 807010304 | bytes 5767168 | tf_op jit(solution)/shard_map/erf,erd->efd/dot_general | solution.py:77
  234.8 1.3 collective-permute-start.1
  236.1 2.0 fusion.16
  238.2 2.1 collective-permute-done.1
  240.3 0.8 fusion.40
  241.0 0.7 fusion.41
  241.7 53.4 %reduce-scatter.5.cloned.1.call-done = f32[256,256]{1,0:T(8,128)} async-done(((f32[2048,256]{1,0:T(8,128)}), f32[256,256]{1,0:T(8,128)}) %reduce-scatter.5.cloned.1.call-update) | async-done | bytes 262160 | tf_op jit(solution)/shard_map/reduce_scatter | solution.py:127
  (64 shorter events, 2.1 us)
Async XLA Ops:
  7.2 77.8 %copy-start = (bf16[1,2048,256]{2,1,0:T(8,128)(2,1)S(1)}, bf16[1,2048,256]{2,1,0:T(8,128)(2,1)}, u32[]{:S(2)}) copy-start(bf16[1,2048,256]{2,1,0:T(8,128)(2,1)} %param.16) | copy-start | bytes 3145732
  7.2 77.8 %all-gather.3.cloned.1.call-start = ((), (), s32[]{:S(2)}) async-start(), calls=%async_computation.6 | async-start | bytes 3932160 | tf_op jit(solution)/shard_map/all_gather | solution.py:66
  80.1 41.6 %all-to-all-start.2 = ((bf16[4,1,768,512]{2,3,1,0:T(8,128)(2,1)}), bf16[4,1,768,512]{2,3,1,0:T(8,128)(2,1)}, u32[]{:S(2)}, u32[]{:S(2)}) async-start(bf16[4,1,768,512]{2,3,1,0:T(8,128)(2,1)} %stack.10), calls=%async_computation.2 | async-start | bytes 6291456 | tf_op jit(solution)/shard_map/all_to_all | solution.py:62
  84.7 4.2 %copy-start.4 = (bf16[1,2048,256]{2,1,0:T(8,128)(2,1)S(1)}, bf16[1,2048,256]{2,1,0:T(8,128)(2,1)}, u32[]{:S(2)}) copy-start(bf16[1,2048,256]{2,1,0:T(8,128)(2,1)} %param.17) | copy-start | bytes 3145732
  84.7 80.2 %reduce-scatter.3.cloned.1.call-start = ((), (), s32[]{:S(2)}) async-start(), calls=%async_computation.7 | async-start | bytes 3932160 | tf_op jit(solution)/shard_map/reduce_scatter | solution.py:92
  85.0 3.9 %copy-start.11 = (bf16[1,768,2048]{2,1,0:T(8,128)(2,1)S(1)}, bf16[1,768,2048]{2,1,0:T(8,128)(2,1)}, u32[]{:S(2)}) copy-start(bf16[1,768,2048]{2,1,0:T(8,128)(2,1)} %all-gather.3.cloned.1.call-done) | copy-start | bytes 9437188
  88.9 32.8 %copy-start.13 = (bf16[1,256,2048]{2,1,0:T(8,128)(2,1)S(1)}, bf16[1,256,2048]{2,1,0:T(8,128)(2,1)}, u32[]{:S(2)}) copy-start(bf16[1,256,2048]{2,1,0:T(8,128)(2,1)} %param.18) | copy-start | bytes 3145732
  125.2 1.0 copy-start.1
  125.2 1.0 copy-start.7
  174.9 25.6 %all-to-all-start.3 = ((bf16[8,2,24576]{2,1,0:T(2,128)(2,1)}), bf16[8,2,24576]{2,1,0:T(2,128)(2,1)S(1)}, u32[]{:S(2)}, u32[]{:S(2)}) async-start(bf16[8,2,24576]{2,1,0:T(2,128)(2,1)} %reshape.228), calls=%async_computation.4 | async-start | bytes 1572864 | tf_op jit(solution)/shard_map/all_to_all | solution.py:96
  180.4 41.6 %all-gather.5.cloned.1.call-start = ((), (), s32[]{:S(2)}) async-start(), calls=%async_computation.8 | async-start | bytes 1310720 | tf_op jit(solution)/shard_map/all_gather | solution.py:103
  203.5 3.8 %copy-start.5 = (bf16[256,256]{1,0:T(8,128)(2,1)S(1)}, bf16[256,256]{1,0:T(8,128)(2,1)}, u32[]{:S(2)}) copy-start(bf16[256,256]{1,0:T(8,128)(2,1)} %param.20) | copy-start | bytes 393220
  203.5 3.8 %copy-start.6 = (bf16[256,256]{1,0:T(8,128)(2,1)S(1)}, bf16[256,256]{1,0:T(8,128)(2,1)}, u32[]{:S(2)}) copy-start(bf16[256,256]{1,0:T(8,128)(2,1)} %param.21) | copy-start | bytes 393220
  203.5 7.0 %copy-start.10 = (bf16[3,256]{1,0:T(4,128)(2,1)S(1)}, bf16[3,256]{1,0:T(4,128)(2,1)}, u32[]{:S(2)}) copy-start(bf16[3,256]{1,0:T(4,128)(2,1)} %param.22) | copy-start | bytes 4612
  203.6 18.5 %copy-start.9 = (bf16[256,256]{1,0:T(8,128)(2,1)S(1)}, bf16[256,256]{1,0:T(8,128)(2,1)}, u32[]{:S(2)}) copy-start(bf16[256,256]{1,0:T(8,128)(2,1)} %param.19) | copy-start | bytes 393220
  207.2 87.9 %reduce-scatter.5.cloned.1.call-start = ((), (), s32[]{:S(2)}) async-start(), calls=%async_computation.9 | async-start | bytes 2359296 | tf_op jit(solution)/shard_map/reduce_scatter | solution.py:127
  207.3 4.5 %collective-permute-start = (f32[2,256]{1,0:T(2,128)S(1)}, f32[2,256]{1,0:T(2,128)S(1)}, u32[]{:S(2)}, u32[]{:S(2)}) collective-permute-start(f32[2,256]{1,0:T(2,128)S(1)} %slice.57), channel_id=1, source_target_pairs={{0,4},{4,8},{8,12},{12,16},{16,20},{20,24},{24,28},{1,5},{5,9},{9,... | collective-permute-start | bytes 6152 | tf_op jit(solution)/shard_map/ppermute | solution.py:10
  222.1 2.7 copy-start.3
  224.8 1.9 copy-start.2
  226.7 4.0 %copy-start.14 = (f32[768,256]{1,0:T(8,128)S(1)}, f32[768,256]{1,0:T(8,128)}, u32[]{:S(2)}) copy-start(f32[768,256]{1,0:T(8,128)} %fusion.4) | copy-start | bytes 2359300
  226.7 4.0 %copy-start.15 = (f32[768,256]{1,0:T(8,128)S(1)}, f32[768,256]{1,0:T(8,128)}, u32[]{:S(2)}) copy-start(f32[768,256]{1,0:T(8,128)} %fusion.6) | copy-start | bytes 2359300
  230.7 5.4 %copy-start.8 = (bf16[768,256]{1,0:T(8,128)(2,1)S(1)}, bf16[768,256]{1,0:T(8,128)(2,1)}, u32[]{:S(2)}) copy-start(bf16[768,256]{1,0:T(8,128)(2,1)} %copy-done.7) | copy-start | bytes 1179652
  230.7 5.4 %copy-start.12 = (bf16[1,768,2048]{2,1,0:T(8,128)(2,1)S(1)}, bf16[1,768,2048]{2,1,0:T(8,128)(2,1)}, u32[]{:S(2)}) copy-start(bf16[1,768,2048]{2,1,0:T(8,128)(2,1)} %all-gather.3.cloned.1.call-done) | copy-start | bytes 9437188
  234.8 5.5 %collective-permute-start.1 = (f32[2,256]{1,0:T(2,128)S(1)}, f32[2,256]{1,0:T(2,128)S(1)}, u32[]{:S(2)}, u32[]{:S(2)}) collective-permute-start(f32[2,256]{1,0:T(2,128)S(1)} %slice.62), channel_id=1, source_target_pairs={{4,0},{8,4},{12,8},{16,12},{20,16},{24,20},{28,24},{5,1},{9,5},{13... | collective-permute-start | bytes 6152 | tf_op jit(solution)/shard_map/ppermute | solution.py:10
Sparse Core Ops, SparseCore 0:
  50.8 27.5 all-gather.2
  129.1 35.7 reduce-scatter.2
  207.3 14.6 all-gather.4
  226.8 68.3 reduce-scatter.4
